TPU v7x, 32 devices: a whole 2x2x4 slice. The times are simulated.
32 devices in a mesh: rep: 2 (over x), fs: 4 (over y, core), tp: 4 (over z).
Axes of the slice: x: 2, y: 2, z: 4, core: 2. Of those that a mesh axis runs over, the one named last changes fastest.
Arguments:
- acts: bfloat16 [2048, 2048], P(('rep', 'fs'), 'tp'), may hold values from -6 to 6
- cotangent: bfloat16 [2048, 2048], P(('rep', 'fs'), 'tp'), may hold values from -8 to 8
- pre_act: bfloat16 [2048, 4096], P(('rep', 'fs'), 'tp'), may hold values from -6 to 6
- up_store: float32 [2048, 4096], P('fs', 'tp'), may hold values from -0.125 to 0.125
- up_scale: float32 [4096], P('tp'), may hold values from 0.5 to 2
- down_store: float32 [4096, 2048], P('tp', 'fs'), may hold values from -0.09375 to 0.09375
- down_scale: float32 [2048], replicated, may hold values from 0.5 to 2
Outputs:
- grad_input: bfloat16 [2048, 2048], P(('rep', 'fs'), 'tp')
- grad_up: float32 [2048, 4096], P('fs', 'tp')
- grad_down: float32 [4096, 2048], P('tp', 'fs')
All inputs are finite; a program needn't handle non-finite values.
Results may differ from a plain program's by a relative error of at most 0.007.
Values may be sent and summed in bfloat16 or wider, within the bound.
No kernel may reach another device: no remote copies, remote signals or barrier semaphores. Data moves between devices by JAX's collectives and lax.ppermute only.
A program may use at most 128 MiB of HBM per device.

v0:
```python
import math
import jax
import jax.numpy as jnp
from jax import lax
from jax.sharding import PartitionSpec as P


def contract_last(left, right):
    return lax.dot_general(
        left, right, (((1,), (1,)), ((), ())), preferred_element_type=jnp.float32
    )


def contract_first(left, right):
    return lax.dot_general(
        left, right, (((0,), (0,)), ((), ())), preferred_element_type=jnp.float32
    )


def body(acts, cotangent, pre_act, up_store, up_scale, down_store, down_scale):
    tok_rows = acts.shape[0]
    norm_factor = 1.0 / math.sqrt(tok_rows * lax.axis_size("fs") * lax.axis_size("rep"))
    full_acts, full_cot = (
        lax.all_gather(acts, "tp", axis=1, tiled=True),
        lax.all_gather(cotangent, "tp", axis=1, tiled=True),
    )
    scaled = (full_cot.astype(jnp.float32) * down_scale[None, :]).astype(jnp.bfloat16)
    down_bf = down_store.astype(jnp.bfloat16)
    up_bf = up_store.astype(jnp.bfloat16)
    d_act = contract_last(scaled, lax.all_gather(down_bf, "fs", axis=1, tiled=True))
    positive = jnp.maximum(pre_act.astype(jnp.float32), 0.0)
    act = (positive * positive).astype(jnp.bfloat16)
    d_pre = (2.0 * positive * d_act * up_scale[None, :]).astype(jnp.bfloat16)
    acts_cols, scaled_cols = (
        lax.all_to_all(full_acts, "fs", split_axis=1, concat_axis=0, tiled=True),
        lax.all_to_all(scaled, "fs", split_axis=1, concat_axis=0, tiled=True),
    )
    act_group, dpre_group = (
        lax.all_gather(act, "fs", axis=0, tiled=True),
        lax.all_gather(d_pre, "fs", axis=0, tiled=True),
    )
    grad_down = contract_first(act_group, scaled_cols) * norm_factor
    grad_up = contract_first(acts_cols, dpre_group) * norm_factor
    partial_value = contract_last(d_pre, lax.all_gather(up_bf, "fs", axis=0, tiled=True))
    grad_input = lax.psum_scatter(partial_value, "tp", scatter_dimension=1, tiled=True).astype(
        jnp.bfloat16
    )
    grad_up, grad_down = lax.psum((grad_up, grad_down), "rep")
    return (grad_input, grad_up, grad_down)


def solution(mesh):
    return jax.shard_map(
        body,
        mesh=mesh,
        in_specs=(
            P(("rep", "fs"), "tp"),
            P(("rep", "fs"), "tp"),
            P(("rep", "fs"), "tp"),
            P("fs", "tp"),
            P("tp"),
            P("tp", "fs"),
            P(),
        ),
        out_specs=(P(("rep", "fs"), "tp"), P("fs", "tp"), P("tp", "fs")),
        check_vma=False,
    )
```

profile of v0, /device:TPU:0, one launch (start us, length us, event | category | flops | bytes accessed | tf_op | source)
XLA Modules:
  0.0 364.8 jit_solution(4651438372138626492)
XLA Ops:
  7.2 0.0 all-gather.7.cloned.1.call-start
  7.2 1.8 copy.12
  9.0 0.0 all-gather.7.cloned.1.call-update
  9.0 0.0 copy-start
  9.0 0.0 all-gather.9.cloned.1.call-start
  9.1 2.8 convert_element_type.27
  11.9 0.0 all-gather.9.cloned.1.call-update
  11.9 0.0 copy-start.3
  12.0 0.0 copy-start.2
  12.0 0.0 all-gather.11.cloned.1.call-start
  12.0 0.0 copy-done
  12.0 1.2 convert_element_type.29
  13.2 0.0 all-gather.11.cloned.1.call-update
  13.2 0.0 all-gather.15.cloned.1.call-start
  13.3 0.0 copy-done.3
  13.3 0.8 copy.13
  14.1 0.0 all-gather.15.cloned.1.call-update
  14.2 0.0 all-gather.17.cloned.1.call-start
  14.2 0.9 multiply_convert_fusion.1
  15.1 0.0 all-gather.17.cloned.1.call-update
  15.2 0.0 all-gather.13.cloned.1.call-start
  15.2 25.6 %all-gather.7.cloned.1.call-done = bf16[256,2048]{0,1:T(8,128)(2,1)} async-done(((bf16[256,512]{0,1:T(8,128)(2,1)}), bf16[256,2048]{0,1:T(8,128)(2,1)}) %all-gather.7.cloned.1.call-update) | async-done | bytes 1048592 | tf_op jit(solution)/shard_map/all_gather | solution.py:25
  40.9 0.0 copy-done.4
  40.9 2.5 multiply_convert_fusion
  43.4 33.5 %all-gather.9.cloned.1.call-done = bf16[1024,2048]{1,0:T(8,128)(2,1)} async-done(((bf16[1024,512]{1,0:T(8,128)(2,1)}), bf16[1024,2048]{1,0:T(8,128)(2,1)}) %all-gather.9.cloned.1.call-update) | async-done | bytes 4194320 | tf_op jit(solution)/shard_map/all_gather | solution.py:30
  76.9 4.7 %fusion.1 = bf16[256,1024]{1,0:T(8,128)(2,1)} fusion(bf16[256,2048]{0,1:T(8,128)(2,1)} %multiply_convert_fusion, bf16[1024,2048]{1,0:T(8,128)(2,1)} %all-gather.9.cloned.1.call-done, bf16[256,1024]{1,0:T(8,128)(2,1)S(1)} %copy-done.2, f32[1024]{0:T(1024)S(1)} %copy-done.5), kind=kOutput, calls=%fused_computation.5 | convolution fusion | flops 1075314688 | bytes 6295552 | tf_op jit(solution)/shard_map/dot_general | solution.py:9
  81.6 0.0 all-gather.13.cloned.1.call-update
  81.6 0.0 reduce-scatter.2.cloned.1.call-start
  81.7 31.2 %all-gather.11.cloned.1.call-done = bf16[2048,1024]{1,0:T(8,128)(2,1)} async-done(((bf16[512,1024]{1,0:T(8,128)(2,1)}), bf16[2048,1024]{1,0:T(8,128)(2,1)}) %all-gather.11.cloned.1.call-update) | async-done | bytes 4194320 | tf_op jit(solution)/shard_map/all_gather | solution.py:44
  112.9 5.0 %fusion.2 = f32[256,2048]{1,0:T(8,128)} fusion(bf16[256,1024]{1,0:T(8,128)(2,1)} %fusion.1, bf16[2048,1024]{1,0:T(8,128)(2,1)} %all-gather.11.cloned.1.call-done), kind=kOutput, calls=%fused_computation.8 | convolution fusion | flops 1073741824 | bytes 6815744 | tf_op jit(solution)/shard_map/dot_general | solution.py:9
  117.9 0.0 reduce-scatter.2.cloned.1.call-update
  117.9 24.4 %all-gather.15.cloned.1.call-done = bf16[256,2048]{0,1:T(8,128)(2,1)} async-done(((bf16[256,512]{0,1:T(8,128)(2,1)}), bf16[256,2048]{0,1:T(8,128)(2,1)}) %all-gather.15.cloned.1.call-update) | async-done | bytes 1048592 | tf_op jit(solution)/shard_map/all_gather | solution.py:24
  142.4 25.7 %all_to_all.38 = bf16[256,4,512]{0,2,1:T(8,128)(2,1)S(1)} all-to-all(bf16[256,4,512]{0,2,1:T(8,128)(2,1)} %bitcast.18), channel_id=1, replica_groups=mesh['rep'=2,'fs'=4,'tp'=4] {'fs'}, dimensions={1} | all-to-all | bytes 2097152 | tf_op jit(solution)/shard_map/all_to_all | solution.py:35
  168.1 3.5 all-to-all-start.1
  171.6 0.0 all-reduce.3.cloned.1.call-start
  171.7 0.5 copy.14
  172.2 17.6 %all-to-all-done.1 = bf16[256,4,512]{0,2,1:T(8,128)(2,1)S(1)} async-done(((bf16[256,4,512]{0,2,1:T(8,128)(2,1)}), bf16[256,4,512]{0,2,1:T(8,128)(2,1)S(1)}, u32[]{:S(2)}, u32[]{:S(2)}) %all-to-all-start.1) | async-done | bytes 1048608 | tf_op jit(solution)/shard_map/all_to_all | solution.py:36
  189.8 0.5 copy.15
  190.3 0.0 all-gather.17.cloned.1.call-done
  190.4 4.3 %convolution_multiply_fusion = f32[1024,512]{1,0:T(8,128)} fusion(bf16[1024,1024]{1,0:T(8,128)(2,1)} %all-gather.17.cloned.1.call-done, bf16[1024,512]{1,0:T(8,128)(2,1)S(1)} %bitcast.20), kind=kOutput, calls=%fused_computation.2 | convolution fusion | flops 1074266112 | bytes 5242880 | tf_op jit(solution)/shard_map/dot_general | solution.py:15
  194.7 4.1 %all-gather.13.cloned.1.call-done = bf16[1024,1024]{1,0:T(8,128)(2,1)} async-done(((bf16[256,1024]{1,0:T(8,128)(2,1)}), bf16[1024,1024]{1,0:T(8,128)(2,1)}) %all-gather.13.cloned.1.call-update) | async-done | bytes 2097168 | tf_op jit(solution)/shard_map/all_gather | solution.py:40
  198.8 4.2 %multiply_bitcast_fusion = f32[512,1024]{0,1:T(8,128)} fusion(bf16[1024,1024]{1,0:T(8,128)(2,1)} %all-gather.13.cloned.1.call-done, bf16[1024,512]{1,0:T(8,128)(2,1)S(1)} %bitcast.19), kind=kOutput, calls=%fused_computation | convolution fusion | flops 1074266112 | bytes 5242880 | tf_op jit(solution)/shard_map/dot_general | solution.py:15
  203.0 0.0 all-reduce.3.cloned.1.call-update
  203.0 40.4 %reduce-scatter.2.cloned.1.call-done = f32[256,512]{1,0:T(8,128)} async-done(((f32[256,2048]{1,0:T(8,128)}), f32[256,512]{1,0:T(8,128)}) %reduce-scatter.2.cloned.1.call-update) | async-done | bytes 524304 | tf_op jit(solution)/shard_map/reduce_scatter | solution.py:45
  243.4 1.8 convert_element_type.30
  245.1 108.4 %all-reduce.3.cloned.1.call-done = (f32[512,1024]{0,1:T(8,128)}, f32[1024,512]{1,0:T(8,128)}) async-done(((f32[512,1024]{0,1:T(8,128)}, f32[1024,512]{1,0:T(8,128)}), (f32[512,1024]{0,1:T(8,128)}, f32[1024,512]{1,0:T(8,128)})) %all-reduce.3.cloned.1.call-update) | async-done | bytes 4194320 | tf_op jit(solution)/shard_map/psum | solution.py:48
  353.6 3.0 copy.16
  356.6 1.3 copy.19
  (6 shorter events, 0.0 us)
Async XLA Ops:
  7.2 33.7 %all-gather.7.cloned.1.call-start = ((), (), s32[]{:S(2)}) async-start(), calls=%async_computation.3 | async-start | bytes 1310720 | tf_op jit(solution)/shard_map/all_gather | solution.py:25
  9.0 3.0 copy-start
  9.0 67.8 %all-gather.9.cloned.1.call-start = ((), (), s32[]{:S(2)}) async-start(), calls=%async_computation.4 | async-start | bytes 5242880 | tf_op jit(solution)/shard_map/all_gather | solution.py:30
  11.9 1.3 copy-start.3
  12.0 2.2 copy-start.2
  12.0 100.9 %all-gather.11.cloned.1.call-start = ((), (), s32[]{:S(2)}) async-start(), calls=%async_computation.5 | async-start | bytes 5242880 | tf_op jit(solution)/shard_map/all_gather | solution.py:44
  13.2 27.7 %copy-start.4 = (f32[2048]{0:T(1024)S(1)}, f32[2048]{0:T(1024)}, u32[]{:S(2)}) copy-start(f32[2048]{0:T(1024)} %param.13) | copy-start | bytes 24580
  13.2 129.1 %all-gather.15.cloned.1.call-start = ((), (), s32[]{:S(2)}) async-start(), calls=%async_computation.8 | async-start | bytes 1310720 | tf_op jit(solution)/shard_map/all_gather | solution.py:24
  14.1 62.7 %copy-start.5 = (f32[1024]{0:T(1024)S(1)}, f32[1024]{0:T(1024)}, u32[]{:S(2)}) copy-start(f32[1024]{0:T(1024)} %param.11) | copy-start | bytes 12292
  14.2 176.2 %all-gather.17.cloned.1.call-start = ((), (), s32[]{:S(2)}) async-start(), calls=%async_computation.9 | async-start | bytes 2621440 | tf_op jit(solution)/shard_map/all_gather | solution.py:39
  15.2 183.6 %all-gather.13.cloned.1.call-start = ((), (), s32[]{:S(2)}) async-start(), calls=%async_computation.7 | async-start | bytes 2621440 | tf_op jit(solution)/shard_map/all_gather | solution.py:40
  81.6 161.8 %reduce-scatter.2.cloned.1.call-start = ((), (), s32[]{:S(2)}) async-start(), calls=%async_computation.6 | async-start | bytes 2621440 | tf_op jit(solution)/shard_map/reduce_scatter | solution.py:45
  168.1 21.7 %all-to-all-start.1 = ((bf16[256,4,512]{0,2,1:T(8,128)(2,1)}), bf16[256,4,512]{0,2,1:T(8,128)(2,1)S(1)}, u32[]{:S(2)}, u32[]{:S(2)}) async-start(bf16[256,4,512]{0,2,1:T(8,128)(2,1)} %bitcast.4), calls=%async_computation.2 | async-start | bytes 2097152 | tf_op jit(solution)/shard_map/all_to_all | solution.py:36
  171.6 182.0 %all-reduce.3.cloned.1.call-start = ((), (), s32[]{:S(2)}) async-start(), calls=%async_computation.10 | async-start | bytes 8388608 | tf_op jit(solution)/shard_map/psum | solution.py:48
  353.6 3.0 copy-start.1
Sparse Core Ops, SparseCore 0:
  10.1 30.6 all-gather.6
  43.0 33.8 all-gather.8
  78.4 34.4 all-gather.10
  114.3 27.9 all-gather.14
  143.8 29.3 all-gather.16
  174.5 24.2 all-gather.12
  201.6 41.6 reduce-scatter.1
  246.4 107.1 all-reduce.2
where the time goes:
time: 365 us
  waiting for transfers between devices  285 us (78%)
  blocking collectives  25.7 us (7%)
  matrix products  18.2 us (5%)
  between operations  14.2 us (4%)
  other arithmetic  9.24 us (3%)
  local copies, waits for them, and re-layouts  8.09 us (2%)
  starting transfers between devices  3.85 us (1%)
    psum x1, waiting for transfers between devices, body(): grad_up, grad_down = lax.psum((grad_up, grad_down), 'rep')  108 us
    reduce_scatter x1, waiting for transfers between devices, body(): lax.psum_scatter(partial_value, 'tp', scatter_dimension=1, tiled=True)  40.4 us
    all_gather x1, waiting for transfers between devices, body(): lax.all_gather(down_bf, 'fs', axis=1, tiled=True)  33.5 us
    all_gather x1, waiting for transfers between devices, body(): lax.all_gather(up_bf, 'fs', axis=0, tiled=True)  31.2 us
    all_to_all x1, blocking collectives, body(): lax.all_to_all(full_acts, 'fs', split_axis=1, concat_axis=0, tiled=True)  25.7 us
    all_gather x1, waiting for transfers between devices, body(): lax.all_gather(cotangent, 'tp', axis=1, tiled=True)  25.6 us
    all_gather x1, waiting for transfers between devices, body(): lax.all_gather(acts, 'tp', axis=1, tiled=True)  24.4 us
    all_to_all x1, waiting for transfers between devices, body(): lax.all_to_all(scaled, 'fs', split_axis=1, concat_axis=0, tiled=True)  17.6 us
  transfers between devices with their start and end apart: 9, of which 8 were waited for; matrix products, arithmetic and copies ran while one was open for 8% of the time, Pallas kernels for 0%

commit v1 on v0

--- a/solution.py
+++ b/solution.py
@@ -21,7 +21,9 @@
     tok_rows = acts.shape[0]
     norm_factor = 1.0 / math.sqrt(tok_rows * lax.axis_size("fs") * lax.axis_size("rep"))
     full_acts, full_cot = (
-        lax.all_gather(acts, "tp", axis=1, tiled=True),
+        jnp.concatenate(
+            lax.all_to_all(jnp.stack([acts] * lax.axis_size("tp")), "tp", 0, 0), axis=1
+        ),
         lax.all_gather(cotangent, "tp", axis=1, tiled=True),
     )
     scaled = (full_cot.astype(jnp.float32) * down_scale[None, :]).astype(jnp.bfloat16)

time: 365 us -> 336 us (0.921)
  waiting for transfers between devices: 285 us -> 232 us
  blocking collectives: 25.7 us -> 51.7 us
    all_to_all x1 -> x2, blocking collectives: 25.7 us -> 51.7 us  [the longest x1 30.6 us: body(): lax.all_to_all(jnp.stack([acts] * lax.axis_size('tp')), 'tp', 0, 0)]
    all_gather x1 -> x0, waiting for transfers between devices: 24.4 us -> none  [body(): lax.all_gather(acts, 'tp', axis=1, tiled=True)]
    reduce_scatter x1, waiting for transfers between devices: 40.4 us -> 21 us  [body(): lax.psum_scatter(partial_value, 'tp', scatter_dimension=1, tiled=True)]
    all_to_all x1, waiting for transfers between devices: 17.6 us -> 9.3 us  [body(): lax.all_to_all(full_acts, 'fs', split_axis=1, concat_axis=0, tiled=True)]
    all_gather x1, waiting for transfers between devices: 4.1 us -> 0.01 us  [body(): lax.all_gather(d_pre, 'fs', axis=0, tiled=True)]
  transfers between devices with their start and end apart: 9 -> 8, of which waited for: 8 -> 6; matrix products, arithmetic and copies ran while one was open for 8% -> 8% of each run, Pallas kernels for 0% -> 0%
where the time goes in v1:
time: 336 us
  waiting for transfers between devices  232 us (69%)
  blocking collectives  51.7 us (15%)
  matrix products  18 us (5%)
  between operations  14.2 us (4%)
  other arithmetic  8.22 us (2%)
  local copies, waits for them, and re-layouts  7.71 us (2%)
  starting transfers between devices  3.8 us (1%)
    psum x1, waiting for transfers between devices, body(): grad_up, grad_down = lax.psum((grad_up, grad_down), 'rep')  108 us
    all_gather x1, waiting for transfers between devices, body(): lax.all_gather(down_bf, 'fs', axis=1, tiled=True)  34.4 us
    all_gather x1, waiting for transfers between devices, body(): lax.all_gather(up_bf, 'fs', axis=0, tiled=True)  32.2 us
    all_to_all x1, blocking collectives, body(): lax.all_to_all(jnp.stack([acts] * lax.axis_size('tp')), 'tp', 0, 0)  30.6 us
    all_gather x1, waiting for transfers between devices, body(): lax.all_gather(cotangent, 'tp', axis=1, tiled=True)  26.6 us
    all_to_all x1, blocking collectives, body(): lax.all_to_all(scaled, 'fs', split_axis=1, concat_axis=0, tiled=True)  21.1 us
    reduce_scatter x1, waiting for transfers between devices, body(): lax.psum_scatter(partial_value, 'tp', scatter_dimension=1, tiled=True)  21 us
    dot_general x2, matrix products, contract_last(): lax.dot_general(left, right, (((1,), (1,)), ((), ())), preferred_element_...  9.31 us
  transfers between devices with their start and end apart: 8, of which 6 were waited for; matrix products, arithmetic and copies ran while one was open for 8% of the time, Pallas kernels for 0%

profile of v1, /device:TPU:0, one launch (start us, length us, event | category | flops | bytes accessed | tf_op | source)
XLA Modules:
  0.0 335.7 jit_solution(15512065897621359785)
XLA Ops:
  7.2 0.0 all-gather.6.cloned.1.call-start
  7.2 1.8 copy.12
  9.0 0.0 all-gather.6.cloned.1.call-update
  9.0 0.0 copy-start
  9.0 0.0 all-gather.8.cloned.1.call-start
  9.1 2.8 convert_element_type.27
  11.9 0.0 all-gather.8.cloned.1.call-update
  11.9 0.0 copy-start.2
  12.0 0.0 all-gather.10.cloned.1.call-start
  12.0 0.0 copy-done
  12.0 1.1 convert_element_type.29
  13.2 0.0 copy-start.4
  13.2 0.0 all-gather.10.cloned.1.call-update
  13.2 0.0 copy-start.5
  13.2 0.0 all-gather.14.cloned.1.call-start
  13.2 0.0 copy-done.2
  13.3 0.9 multiply_convert_fusion.1
  14.2 0.0 all-gather.14.cloned.1.call-update
  14.2 0.0 all-gather.12.cloned.1.call-start
  14.2 26.6 %all-gather.6.cloned.1.call-done = bf16[256,2048]{0,1:T(8,128)(2,1)} async-done(((bf16[256,512]{0,1:T(8,128)(2,1)}), bf16[256,2048]{0,1:T(8,128)(2,1)}) %all-gather.6.cloned.1.call-update) | async-done | bytes 1048592 | tf_op jit(solution)/shard_map/all_gather | solution.py:27
  40.9 0.0 copy-done.4
  40.9 1.6 multiply_convert_fusion
  42.4 34.4 %all-gather.8.cloned.1.call-done = bf16[1024,2048]{1,0:T(8,128)(2,1)} async-done(((bf16[1024,512]{1,0:T(8,128)(2,1)}), bf16[1024,2048]{1,0:T(8,128)(2,1)}) %all-gather.8.cloned.1.call-update) | async-done | bytes 4194320 | tf_op jit(solution)/shard_map/all_gather | solution.py:32
  76.9 0.0 copy-done.5
  76.9 4.4 %fusion.1 = bf16[256,1024]{1,0:T(8,128)(2,1)} fusion(bf16[256,2048]{0,1:T(8,128)(2,1)S(1)} %multiply_convert_fusion, bf16[1024,2048]{1,0:T(8,128)(2,1)} %all-gather.8.cloned.1.call-done, bf16[256,1024]{1,0:T(8,128)(2,1)S(1)} %copy-done.2, f32[1024]{0:T(1024)S(1)} %copy-done.5), kind=kOutput, calls=%fused_computation.5 | convolution fusion | flops 1075314688 | bytes 6295552 | tf_op jit(solution)/shard_map/dot_general | solution.py:9
  81.2 0.0 all-gather.12.cloned.1.call-update
  81.2 0.0 reduce-scatter.2.cloned.1.call-start
  81.3 32.2 %all-gather.10.cloned.1.call-done = bf16[2048,1024]{1,0:T(8,128)(2,1)} async-done(((bf16[512,1024]{1,0:T(8,128)(2,1)}), bf16[2048,1024]{1,0:T(8,128)(2,1)}) %all-gather.10.cloned.1.call-update) | async-done | bytes 4194320 | tf_op jit(solution)/shard_map/all_gather | solution.py:46
  113.5 5.0 %fusion.2 = f32[256,2048]{1,0:T(8,128)} fusion(bf16[256,1024]{1,0:T(8,128)(2,1)} %fusion.1, bf16[2048,1024]{1,0:T(8,128)(2,1)} %all-gather.10.cloned.1.call-done), kind=kOutput, calls=%fused_computation.8 | convolution fusion | flops 1073741824 | bytes 6815744 | tf_op jit(solution)/shard_map/dot_general | solution.py:9
  118.5 0.0 reduce-scatter.2.cloned.1.call-update
  118.5 0.9 copy-done.3
  119.4 0.1 stack.2
  119.5 30.6 %all_to_all.40 = bf16[4,256,512]{2,1,0:T(8,128)(2,1)} all-to-all(bf16[4,256,512]{2,1,0:T(8,128)(2,1)S(1)} %stack.2), channel_id=1, replica_groups=mesh['rep'=2,'fs'=4,'tp'=4] {'tp'}, dimensions={0} | all-to-all | bytes 2097152 | tf_op jit(solution)/shard_map/all_to_all | solution.py:25
  150.1 21.1 %all_to_all.41 = bf16[256,4,512]{0,2,1:T(8,128)(2,1)S(1)} all-to-all(bf16[256,4,512]{0,2,1:T(8,128)(2,1)S(1)} %bitcast.17), channel_id=1, replica_groups=mesh['rep'=2,'fs'=4,'tp'=4] {'fs'}, dimensions={1} | all-to-all | bytes 2097152 | tf_op jit(solution)/shard_map/all_to_all | solution.py:38
  171.2 3.5 %all-to-all-start.1 = ((bf16[256,4,512]{2,0,1:T(8,128)(2,1)}), bf16[256,4,512]{2,0,1:T(8,128)(2,1)S(1)}, u32[]{:S(2)}, u32[]{:S(2)}) async-start(bf16[256,4,512]{2,0,1:T(8,128)(2,1)} %bitcast), calls=%async_computation.2 | async-start | bytes 2097152 | tf_op jit(solution)/shard_map/all_to_all | solution.py:37
  174.7 0.0 all-reduce.3.cloned.1.call-start
  174.8 0.5 copy.13
  175.3 0.0 all-gather.14.cloned.1.call-done
  175.4 4.5 %convolution_multiply_fusion = f32[1024,512]{1,0:T(8,128)} fusion(bf16[1024,1024]{1,0:T(8,128)(2,1)} %all-gather.14.cloned.1.call-done, bf16[1024,512]{1,0:T(8,128)(2,1)S(1)} %bitcast.20), kind=kOutput, calls=%fused_computation.2 | convolution fusion | flops 1074266112 | bytes 5242880 | tf_op jit(solution)/shard_map/dot_general | solution.py:15
  179.8 9.3 %all-to-all-done.1 = bf16[256,4,512]{2,0,1:T(8,128)(2,1)S(1)} async-done(((bf16[256,4,512]{2,0,1:T(8,128)(2,1)}), bf16[256,4,512]{2,0,1:T(8,128)(2,1)S(1)}, u32[]{:S(2)}, u32[]{:S(2)}) %all-to-all-start.1) | async-done | bytes 1048608 | tf_op jit(solution)/shard_map/all_to_all | solution.py:37
  189.1 4.2 %multiply_bitcast_fusion = f32[512,1024]{0,1:T(8,128)} fusion(bf16[1024,1024]{1,0:T(8,128)(2,1)} %all-gather.12.cloned.1.call-done, bf16[1024,512]{1,0:T(8,128)(2,1)S(1)} %bitcast.19), kind=kOutput, calls=%fused_computation | convolution fusion | flops 1074266112 | bytes 5242880 | tf_op jit(solution)/shard_map/dot_general | solution.py:15
  193.3 0.0 all-reduce.3.cloned.1.call-update
  193.4 21.0 %reduce-scatter.2.cloned.1.call-done = f32[256,512]{1,0:T(8,128)} async-done(((f32[256,2048]{1,0:T(8,128)}), f32[256,512]{1,0:T(8,128)}) %reduce-scatter.2.cloned.1.call-update) | async-done | bytes 524304 | tf_op jit(solution)/shard_map/reduce_scatter | solution.py:47
  214.3 1.8 convert_element_type.30
  216.1 108.4 %all-reduce.3.cloned.1.call-done = (f32[512,1024]{0,1:T(8,128)}, f32[1024,512]{1,0:T(8,128)}) async-done(((f32[512,1024]{0,1:T(8,128)}, f32[1024,512]{1,0:T(8,128)}), (f32[512,1024]{0,1:T(8,128)}, f32[1024,512]{1,0:T(8,128)})) %all-reduce.3.cloned.1.call-update) | async-done | bytes 4194320 | tf_op jit(solution)/shard_map/psum | solution.py:50
  324.5 3.0 copy.14
  327.6 0.0 copy-done.1
  327.6 1.3 copy.17
  (3 shorter events, 0.0 us)
Async XLA Ops:
  7.2 33.7 %all-gather.6.cloned.1.call-start = ((), (), s32[]{:S(2)}) async-start(), calls=%async_computation.4 | async-start | bytes 1310720 | tf_op jit(solution)/shard_map/all_gather | solution.py:27
  9.0 3.0 copy-start
  9.0 67.8 %all-gather.8.cloned.1.call-start = ((), (), s32[]{:S(2)}) async-start(), calls=%async_computation.5 | async-start | bytes 5242880 | tf_op jit(solution)/shard_map/all_gather | solution.py:32
  11.9 1.3 copy-start.2
  12.0 101.5 %all-gather.10.cloned.1.call-start = ((), (), s32[]{:S(2)}) async-start(), calls=%async_computation.6 | async-start | bytes 5242880 | tf_op jit(solution)/shard_map/all_gather | solution.py:46
  13.2 27.7 %copy-start.4 = (f32[2048]{0:T(1024)S(1)}, f32[2048]{0:T(1024)}, u32[]{:S(2)}) copy-start(f32[2048]{0:T(1024)} %param.13) | copy-start | bytes 24580
  13.2 63.7 %copy-start.5 = (f32[1024]{0:T(1024)S(1)}, f32[1024]{0:T(1024)}, u32[]{:S(2)}) copy-start(f32[1024]{0:T(1024)} %param.11) | copy-start | bytes 12292
  13.2 162.2 %all-gather.14.cloned.1.call-start = ((), (), s32[]{:S(2)}) async-start(), calls=%async_computation.9 | async-start | bytes 2621440 | tf_op jit(solution)/shard_map/all_gather | solution.py:41
  14.2 174.9 %all-gather.12.cloned.1.call-start = ((), (), s32[]{:S(2)}) async-start(), calls=%async_computation.8 | async-start | bytes 2621440 | tf_op jit(solution)/shard_map/all_gather | solution.py:42
  81.2 133.1 %reduce-scatter.2.cloned.1.call-start = ((), (), s32[]{:S(2)}) async-start(), calls=%async_computation.7 | async-start | bytes 2621440 | tf_op jit(solution)/shard_map/reduce_scatter | solution.py:47
  118.5 0.9 copy-start.3
  171.2 17.9 %all-to-all-start.1 = ((bf16[256,4,512]{2,0,1:T(8,128)(2,1)}), bf16[256,4,512]{2,0,1:T(8,128)(2,1)S(1)}, u32[]{:S(2)}, u32[]{:S(2)}) async-start(bf16[256,4,512]{2,0,1:T(8,128)(2,1)} %bitcast), calls=%async_computation.2 | async-start | bytes 2097152 | tf_op jit(solution)/shard_map/all_to_all | solution.py:37
  174.7 149.8 %all-reduce.3.cloned.1.call-start = ((), (), s32[]{:S(2)}) async-start(), calls=%async_computation.10 | async-start | bytes 8388608 | tf_op jit(solution)/shard_map/psum | solution.py:50
  324.5 3.0 copy-start.1
Sparse Core Ops, SparseCore 0:
  10.1 30.6 all-gather.5
  43.0 33.8 all-gather.7
  79.0 34.4 all-gather.9
  114.9 22.5 all-gather.13
  138.9 26.8 all-gather.11
  168.5 45.7 reduce-scatter.1
  217.4 107.1 all-reduce.2
